TPU v7x, 32 devices: a whole 2x2x4 slice. The times are simulated.
32 devices in a mesh: gr: 2 (over x), fs: 8 (over z, y), tp: 2 (over core).
Axes of the slice: x: 2, y: 2, z: 4, core: 2. Of those that a mesh axis runs over, the one named last changes fastest.
Arguments:
- tokens: bfloat16 [4096, 2048], P(('gr', 'tp'), 'fs'), may hold values from -400 to 400
- norm_gain: float32 [2048], P('fs'), may hold values from 0.1 to 1.9
- up_weight: float32 [2048, 8192], P('fs', ('gr', 'tp')), may hold values from -0.125 to 0.125
- down_weight: float32 [8192, 2048], P('fs', ('gr', 'tp')), may hold values from -0.09375 to 0.09375
Outputs:
- mixed: bfloat16 [2048, 4096], P('fs', ('gr', 'tp'))
- up_ready: bfloat16 [2048, 8192], P(None, 'fs')
- down_ready: bfloat16 [8192, 2048], P('fs')
All inputs are finite; a program needn't handle non-finite values.
Results may differ from a plain program's by a relative error of at most 0.023.
Values may be sent and summed in bfloat16 or wider, within the bound.
No kernel may reach another device: no remote copies, remote signals or barrier semaphores. Data moves between devices by JAX's collectives and lax.ppermute only.
A program may use at most 64 MiB of HBM per device.

v0:
```python
import jax
import jax.numpy as jnp
from jax import lax
from jax.sharding import PartitionSpec as P

epsilon = 1e-06


def shards(tokens, norm_gain, up_weight, down_weight):
    folded = (norm_gain[:, None] * up_weight).astype(jnp.bfloat16)
    down_cast = down_weight.astype(jnp.bfloat16)
    fs_count = lax.axis_size("fs")
    group_count = lax.axis_size(("gr", "tp"))
    rows_here, cols_here = folded.shape
    sub_rows = rows_here // group_count
    row_groups = folded.reshape(group_count, sub_rows, cols_here)
    full_rows = lax.all_to_all(row_groups, ("gr", "tp"), split_axis=0, concat_axis=2, tiled=True)
    full_width = full_rows.shape[2]
    unit_width = full_width // fs_count
    by_unit = full_rows.reshape(1, sub_rows, fs_count, unit_width)
    by_owner = lax.all_to_all(by_unit, "fs", split_axis=2, concat_axis=0, tiled=True)
    arranged = by_owner.reshape(fs_count, 1, sub_rows, unit_width)
    stacked, down_full = (
        lax.all_gather(arranged, ("gr", "tp"), axis=1, tiled=True),
        lax.all_gather(down_cast, ("gr", "tp"), axis=1, tiled=True),
    )
    up_full = stacked.reshape(fs_count * group_count * sub_rows, unit_width)
    model_width = up_full.shape[0]
    piece = lax.all_gather(tokens, "fs", axis=1, tiled=True)
    running = jnp.dot(piece, up_full, preferred_element_type=jnp.float32)
    piece_wide = piece.astype(jnp.float32)
    squares = jnp.sum(piece_wide * piece_wide, axis=1)
    raw_up, squares = (running, squares)
    row_scale = lax.rsqrt(squares / model_width + epsilon)
    hidden = jnp.square(jax.nn.relu(raw_up * row_scale[:, None])).astype(jnp.bfloat16)
    outcome = lax.psum_scatter(
        lax.dot_general(
            down_full, hidden, (((0,), (1,)), ((), ())), preferred_element_type=jnp.float32
        ).astype(jnp.bfloat16),
        "fs",
        scatter_dimension=0,
        tiled=True,
    )
    return (outcome, up_full, down_full)


def solution(mesh):
    in_specs = (P(("gr", "tp"), "fs"), P("fs"), P("fs", ("gr", "tp")), P("fs", ("gr", "tp")))
    out_specs = (P("fs", ("gr", "tp")), P(None, "fs"), P("fs", None))
    return jax.shard_map(shards, mesh=mesh, in_specs=in_specs, out_specs=out_specs, check_vma=False)
```

profile of v0, /device:TPU:0, one launch (start us, length us, event | category | flops | bytes accessed | tf_op | source)
XLA Modules:
  0.0 292.2 jit_solution(18041260175511250311)
XLA Ops:
  7.2 0.0 all-gather.5.cloned.1.call-start
  7.2 0.7 all-gather.5.cloned.1.call-update
  7.9 0.0 all-gather.9.cloned.1.call-start
  7.9 1.8 multiply_convert_fusion.1
  9.7 18.5 %all_to_all.30 = bf16[4,64,2048]{2,1,0:T(8,128)(2,1)S(1)} all-to-all(bf16[4,64,2048]{2,1,0:T(8,128)(2,1)S(1)} %bitcast.19), channel_id=1, replica_groups=mesh['gr'=2,'fs'=8,'tp'=2] {'gr','tp'}, dimensions={0} | all-to-all | bytes 2097152 | tf_op jit(solution)/shard_map/all_to_all | solution.py:17
  28.2 0.8 copy.13
  29.0 0.3 reshape.27
  29.3 0.6 copy.14
  29.9 53.7 %all_to_all.31 = bf16[1,64,8,1024]{3,1,0,2:T(8,128)(2,1)} all-to-all(bf16[1,64,8,1024]{3,1,0,2:T(8,128)(2,1)S(1)} %copy.14), channel_id=1, replica_groups=mesh['gr'=2,'fs'=8,'tp'=2] {'fs'}, dimensions={2} | all-to-all | bytes 2097152 | tf_op jit(solution)/shard_map/all_to_all | solution.py:21
  83.6 0.0 all-gather.9.cloned.1.call-update
  83.6 0.0 all-gather.7.cloned.1.call-start
  83.7 1.1 convert_element_type.22
  84.8 0.0 all-gather.7.cloned.1.call-update
  84.8 0.0 reduce-scatter.2.cloned.1.call-start
  84.9 18.0 %all-gather.5.cloned.1.call-done = bf16[1024,2048]{1,0:T(8,128)(2,1)} async-done(((bf16[1024,256]{1,0:T(8,128)(2,1)}), bf16[1024,2048]{1,0:T(8,128)(2,1)}) %all-gather.5.cloned.1.call-update) | async-done | bytes 4194320 | tf_op jit(solution)/shard_map/all_gather | solution.py:29
  102.8 3.1 %multiply_reduce_fusion = f32[1024]{0:T(1024)S(1)} fusion(bf16[1024,2048]{1,0:T(8,128)(2,1)} %all-gather.5.cloned.1.call-done), kind=kLoop, calls=%fused_computation | loop fusion | flops 6290432 | bytes 4198400 | tf_op jit(solution)/shard_map/reduce_sum | solution.py:32
  105.9 32.9 %all-gather.9.cloned.1.call-done = bf16[8,4,64,1,1024]{4,2,3,0,1:T(8,128)(2,1)} async-done(((bf16[8,1,64,1,1024]{4,2,3,0,1:T(8,128)(2,1)}), bf16[8,4,64,1,1024]{4,2,3,0,1:T(8,128)(2,1)}) %all-gather.9.cloned.1.call-update) | async-done | bytes 4194320 | tf_op jit(solution)/shard_map/all_gather | solution.py:24
  138.8 4.9 %copy.16 = bf16[8,4,64,1,1024]{4,2,1,0,3:T(8,128)(2,1)} copy(bf16[8,4,64,1,1024]{4,2,3,0,1:T(8,128)(2,1)} %all-gather.9.cloned.1.call-done) | data formatting | bytes 8388608 | tf_op jit(solution)/shard_map/all_gather | solution.py:24
  143.7 31.7 %all-gather.7.cloned.1.call-done = bf16[1024,2048]{1,0:T(8,128)(2,1)} async-done(((bf16[1024,512]{1,0:T(8,128)(2,1)}), bf16[1024,2048]{1,0:T(8,128)(2,1)}) %all-gather.7.cloned.1.call-update) | async-done | bytes 4194320 | tf_op jit(solution)/shard_map/all_gather | solution.py:25
  175.5 14.5 %convert_bitcast_fusion = bf16[2048,1024]{0,1:T(8,128)(2,1)} fusion(bf16[1024,2048]{1,0:T(8,128)(2,1)} %all-gather.7.cloned.1.call-done, bf16[2048,1024]{1,0:T(8,128)(2,1)} %bitcast.15, bf16[1024,2048]{1,0:T(8,128)(2,1)} %all-gather.5.cloned.1.call-done, f32[1024]{0:T(1024)S(1)} %add_rsqrt_fusion), kind=kOutput, calls=%fused_computation.1 | convolution fusion | flops 8596226048 | bytes 16781312 | tf_op jit(solution)/shard_map/dot_general | solution.py:37
  190.0 0.0 reduce-scatter.2.cloned.1.call-update
  190.0 88.8 %reduce-scatter.2.cloned.1.call-done = bf16[256,1024]{0,1:T(8,128)(2,1)} async-done(((bf16[2048,1024]{0,1:T(8,128)(2,1)}), bf16[256,1024]{0,1:T(8,128)(2,1)}) %reduce-scatter.2.cloned.1.call-update) | async-done | bytes 524304 | tf_op jit(solution)/shard_map/reduce_scatter | solution.py:36
  278.8 2.0 copy.17
  280.9 4.8 %copy.19 = bf16[1024,2048]{1,0:T(8,128)(2,1)} copy(bf16[1024,2048]{1,0:T(8,128)(2,1)} %all-gather.7.cloned.1.call-done) | data formatting | bytes 8388608
  (3 shorter events, 0.0 us)
Async XLA Ops:
  7.2 95.7 %all-gather.5.cloned.1.call-start = ((), (), s32[]{:S(2)}) async-start(), calls=%async_computation.3 | async-start | bytes 4718592 | tf_op jit(solution)/shard_map/all_gather | solution.py:29
  7.9 130.9 %all-gather.9.cloned.1.call-start = ((), (), s32[]{:S(2)}) async-start(), calls=%async_computation.6 | async-start | bytes 5242880 | tf_op jit(solution)/shard_map/all_gather | solution.py:24
  29.9 53.8 %copy-start = (f32[1024,512]{1,0:T(8,128)S(1)}, f32[1024,512]{1,0:T(8,128)}, u32[]{:S(2)}) copy-start(f32[1024,512]{1,0:T(8,128)} %param.7) | copy-start | bytes 6291460
  83.6 91.8 %all-gather.7.cloned.1.call-start = ((), (), s32[]{:S(2)}) async-start(), calls=%async_computation.4 | async-start | bytes 5242880 | tf_op jit(solution)/shard_map/all_gather | solution.py:25
  84.8 194.0 %reduce-scatter.2.cloned.1.call-start = ((), (), s32[]{:S(2)}) async-start(), calls=%async_computation.5 | async-start | bytes 4718592 | tf_op jit(solution)/shard_map/reduce_scatter | solution.py:36
Sparse Core Ops, SparseCore 0:
  10.0 92.7 all-gather.4
  104.4 34.3 all-gather.8
  141.0 34.4 all-gather.6
  190.1 88.6 reduce-scatter.1
where the time goes:
time: 293 us; the launch traced here: 292 us
  waiting for transfers between devices  172 us (59%)
  blocking collectives  72.2 us (25%)
  matrix products  14.5 us (5%)
  between operations  13.8 us (5%)
  local copies, waits for them, and re-layouts  13.4 us (5%)
  other arithmetic  5.95 us (2%)
    reduce_scatter x1, waiting for transfers between devices, shards(): lax.psum_scatter(lax.dot_general(down_full, hidden, (((0,), (1,)), ((), (...  88.8 us
    all_to_all x1, blocking collectives, shards(): lax.all_to_all(by_unit, 'fs', split_axis=2, concat_axis=0, tiled=True)  53.7 us
    all_gather x1, waiting for transfers between devices, shards(): lax.all_gather(arranged, ('gr', 'tp'), axis=1, tiled=True)  32.9 us
    all_gather x1, waiting for transfers between devices, shards(): lax.all_gather(down_cast, ('gr', 'tp'), axis=1, tiled=True)  31.7 us
    all_to_all x1, blocking collectives, shards(): lax.all_to_all(row_groups, ('gr', 'tp'), split_axis=0, concat_axis=2, til...  18.5 us
    all_gather x1, waiting for transfers between devices, shards(): piece = lax.all_gather(tokens, 'fs', axis=1, tiled=True)  18 us
    dot_general x1, matrix products, shards(): lax.dot_general(down_full, hidden, (((0,), (1,)), ((), ())), preferred_el...  14.5 us
    unnamed x4, local copies, waits for them, and re-layouts  6.83 us
  transfers between devices with their start and end apart: 4, of which 4 were waited for; matrix products, arithmetic and copies ran while one was open for 4% of the time, Pallas kernels for 0%

commit v1 on v0

--- a/solution.py
+++ b/solution.py
@@ -4,6 +4,11 @@
 from jax.sharding import PartitionSpec as P
 
 epsilon = 1e-06
+
+
+def gather_over(x, mesh_axis, d):
+    sent = jnp.stack([x] * lax.axis_size(mesh_axis))
+    return jnp.concatenate(lax.all_to_all(sent, mesh_axis, 0, 0), axis=d)
 
 
 def shards(tokens, norm_gain, up_weight, down_weight):
@@ -22,7 +27,7 @@
     arranged = by_owner.reshape(fs_count, 1, sub_rows, unit_width)
     stacked, down_full = (
         lax.all_gather(arranged, ("gr", "tp"), axis=1, tiled=True),
-        lax.all_gather(down_cast, ("gr", "tp"), axis=1, tiled=True),
+        gather_over(down_cast, ("gr", "tp"), 1),
     )
     up_full = stacked.reshape(fs_count * group_count * sub_rows, unit_width)
     model_width = up_full.shape[0]

time: 293 us -> 280 us (0.956)
  waiting for transfers between devices: 172 us -> 79.4 us
  blocking collectives: 72.2 us -> 145 us
  local copies, waits for them, and re-layouts: 13.4 us -> 21.7 us
    all_to_all x0 -> x1, blocking collectives: none -> 73.1 us  [gather_over(): return jnp.concatenate(lax.all_to_all(sent, mesh_axis, 0, 0), axis=d)]
    all_gather x1, waiting for transfers between devices: 32.9 us -> 0.02 us  [shards(): lax.all_gather(arranged, ('gr', 'tp'), axis=1, tiled=True)]
    all_gather x1 -> x0, waiting for transfers between devices: 31.7 us -> none  [shards(): lax.all_gather(down_cast, ('gr', 'tp'), axis=1, tiled=True)]
    all_gather x1, waiting for transfers between devices: 18 us -> 0.01 us  [shards(): piece = lax.all_gather(tokens, 'fs', axis=1, tiled=True)]
    reduce_scatter x1, waiting for transfers between devices: 88.8 us -> 78.7 us  [shards(): lax.psum_scatter(lax.dot_general(down_full, hidden, (((0,), (1,)), ((), (...]
    all_to_all x0 -> x1, local copies, waits for them, and re-layouts: none -> 6.33 us  [gather_over(): return jnp.concatenate(lax.all_to_all(sent, mesh_axis, 0, 0), axis=d)]
  transfers between devices with their start and end apart: 4 -> 3, of which waited for: 4 -> 1; matrix products, arithmetic and copies ran while one was open for 4% -> 7% of each run, Pallas kernels for 0% -> 0%
where the time goes in v1:
time: 280 us
  blocking collectives  145 us (52%)
  waiting for transfers between devices  79.4 us (28%)
  local copies, waits for them, and re-layouts  21.7 us (8%)
  matrix products  14.5 us (5%)
  between operations  13.8 us (5%)
  other arithmetic  4.98 us (2%)
    reduce_scatter x1, waiting for transfers between devices, shards(): lax.psum_scatter(lax.dot_general(down_full, hidden, (((0,), (1,)), ((), (...  78.7 us
    all_to_all x1, blocking collectives, gather_over(): return jnp.concatenate(lax.all_to_all(sent, mesh_axis, 0, 0), axis=d)  73.1 us
    all_to_all x1, blocking collectives, shards(): lax.all_to_all(by_unit, 'fs', split_axis=2, concat_axis=0, tiled=True)  53.7 us
    all_to_all x1, blocking collectives, shards(): lax.all_to_all(row_groups, ('gr', 'tp'), split_axis=0, concat_axis=2, til...  18.5 us
    dot_general x1, matrix products, shards(): lax.dot_general(down_full, hidden, (((0,), (1,)), ((), ())), preferred_el...  14.5 us
    unnamed x4, local copies, waits for them, and re-layouts  8.48 us
    all_to_all x1, local copies, waits for them, and re-layouts, gather_over(): return jnp.concatenate(lax.all_to_all(sent, mesh_axis, 0, 0), axis=d)  6.33 us
  transfers between devices with their start and end apart: 3, of which 1 were waited for; matrix products, arithmetic and copies ran while one was open for 7% of the time, Pallas kernels for 0%

profile of v1, /device:TPU:0, one launch (start us, length us, event | category | flops | bytes accessed | tf_op | source)
XLA Modules:
  0.0 279.8 jit_solution(8483847400617460806)
XLA Ops:
  7.2 0.0 all-gather.4.cloned.1.call-start
  7.2 0.7 all-gather.4.cloned.1.call-update
  7.9 0.0 all-gather.6.cloned.1.call-start
  7.9 1.8 multiply_convert_fusion.1
  9.7 18.5 %all_to_all.35 = bf16[4,64,2048]{2,1,0:T(8,128)(2,1)S(1)} all-to-all(bf16[4,64,2048]{2,1,0:T(8,128)(2,1)S(1)} %bitcast.24), channel_id=1, replica_groups=mesh['gr'=2,'fs'=8,'tp'=2] {'gr','tp'}, dimensions={0} | all-to-all | bytes 2097152 | tf_op jit(solution)/shard_map/all_to_all | solution.py:22
  28.2 0.8 copy.18
  29.0 0.3 reshape.35
  29.3 0.6 copy.19
  29.9 0.0 copy-start
  29.9 53.7 %all_to_all.36 = bf16[1,64,8,1024]{3,1,0,2:T(8,128)(2,1)} all-to-all(bf16[1,64,8,1024]{3,1,0,2:T(8,128)(2,1)S(1)} %copy.19), channel_id=1, replica_groups=mesh['gr'=2,'fs'=8,'tp'=2] {'fs'}, dimensions={2} | all-to-all | bytes 2097152 | tf_op jit(solution)/shard_map/all_to_all | solution.py:26
  83.6 0.0 all-gather.6.cloned.1.call-update
  83.6 0.0 reduce-scatter.2.cloned.1.call-start
  83.7 0.1 convert_element_type.22
  83.8 0.3 stack.2
  84.2 73.1 %all_to_all.37 = bf16[4,1024,512]{2,1,0:T(8,128)(2,1)} all-to-all(bf16[4,1024,512]{2,1,0:T(8,128)(2,1)S(1)} %stack.2), channel_id=1, replica_groups=mesh['gr'=2,'fs'=8,'tp'=2] {'gr','tp'}, dimensions={0} | all-to-all | bytes 8388608 | tf_op jit(solution)/shard_map/all_to_all | solution.py:11
  157.2 6.3 %copy.22 = bf16[4,1024,512]{1,2,0:T(8,128)(2,1)} copy(bf16[4,1024,512]{2,1,0:T(8,128)(2,1)} %all_to_all.37) | data formatting | bytes 8388608 | tf_op jit(solution)/shard_map/all_to_all | solution.py:11
  163.6 3.1 %multiply_reduce_fusion = f32[1024]{0:T(1024)S(1)} fusion(bf16[1024,2048]{1,0:T(8,128)(2,1)} %all-gather.4.cloned.1.call-done), kind=kLoop, calls=%fused_computation | loop fusion | flops 6290432 | bytes 4198400 | tf_op jit(solution)/shard_map/reduce_sum | solution.py:37
  166.6 0.0 all-gather.6.cloned.1.call-done
  166.7 4.9 %copy.21 = bf16[8,4,64,1,1024]{4,2,1,0,3:T(8,128)(2,1)} copy(bf16[8,4,64,1,1024]{4,2,3,0,1:T(8,128)(2,1)} %all-gather.6.cloned.1.call-done) | data formatting | bytes 8388608 | tf_op jit(solution)/shard_map/all_gather | solution.py:29
  171.6 14.5 %convert_bitcast_fusion = bf16[2048,1024]{0,1:T(8,128)(2,1)} fusion(bf16[1024,2048]{0,1:T(8,128)(2,1)} %bitcast.18, bf16[2048,1024]{1,0:T(8,128)(2,1)} %bitcast.20, bf16[1024,2048]{1,0:T(8,128)(2,1)} %all-gather.4.cloned.1.call-done, f32[1024]{0:T(1024)S(1)} %add_rsqrt_fusion), kind=kOutput, calls=%fused_computation.1 | convolution fusion | flops 8596226048 | bytes 16781312 | tf_op jit(solution)/shard_map/dot_general | solution.py:42
  186.1 0.0 reduce-scatter.2.cloned.1.call-update
  186.1 6.4 %copy.24 = bf16[1024,2048]{1,0:T(8,128)(2,1)} copy(bf16[1024,2048]{0,1:T(8,128)(2,1)} %bitcast.19) | data formatting | bytes 8388608
  192.5 78.7 %reduce-scatter.2.cloned.1.call-done = bf16[256,1024]{0,1:T(8,128)(2,1)} async-done(((bf16[2048,1024]{0,1:T(8,128)(2,1)}), bf16[256,1024]{0,1:T(8,128)(2,1)}) %reduce-scatter.2.cloned.1.call-update) | async-done | bytes 524304 | tf_op jit(solution)/shard_map/reduce_scatter | solution.py:41
  271.2 2.0 copy.23
  (3 shorter events, 0.0 us)
Async XLA Ops:
  7.2 156.4 %all-gather.4.cloned.1.call-start = ((), (), s32[]{:S(2)}) async-start(), calls=%async_computation.4 | async-start | bytes 4718592 | tf_op jit(solution)/shard_map/all_gather | solution.py:34
  7.9 158.8 %all-gather.6.cloned.1.call-start = ((), (), s32[]{:S(2)}) async-start(), calls=%async_computation.6 | async-start | bytes 5242880 | tf_op jit(solution)/shard_map/all_gather | solution.py:29
  29.9 53.8 %copy-start = (f32[1024,512]{1,0:T(8,128)S(1)}, f32[1024,512]{1,0:T(8,128)}, u32[]{:S(2)}) copy-start(f32[1024,512]{1,0:T(8,128)} %param.7) | copy-start | bytes 6291460
  83.6 187.6 %reduce-scatter.2.cloned.1.call-start = ((), (), s32[]{:S(2)}) async-start(), calls=%async_computation.5 | async-start | bytes 4718592 | tf_op jit(solution)/shard_map/reduce_scatter | solution.py:41
Sparse Core Ops, SparseCore 0:
  10.0 92.7 all-gather.3
  104.4 55.3 all-gather.5
  186.2 84.9 reduce-scatter.1
